TPU v7x, 32 devices: a whole 2x2x4 slice. The times are simulated.
32 devices in a mesh: sp: 8 (over z, y), dp: 4 (over x, core).
Axes of the slice: x: 2, y: 2, z: 4, core: 2. Of those that a mesh axis runs over, the one named last changes fastest.
Arguments:
- stream: bfloat16 [4, 1024, 2048], P('dp', 'sp'), may hold values from -6 to 6
- queries: bfloat16 [4, 1024, 1024], P('dp', 'sp'), may hold values from -6 to 6
- keys_in: bfloat16 [4, 1024, 1024], P('dp', 'sp'), may hold values from -6 to 6
- values_in: bfloat16 [4, 1024, 1024], P('dp', 'sp'), may hold values from -6 to 6
- key_shift: bfloat16 [4, 1024, 16], P('dp', 'sp'), may hold values from -8 to 16
- head_shift: float32 [16], replicated, may hold values from -16 to 0
- mix_gain: float32 [1024], replicated, may hold values from 0.1 to 1.9
- out_weight: bfloat16 [1024, 2048], replicated, may hold values from -0.1875 to 0.1875
- post_gain: float32 [2048], replicated, may hold values from 0.1 to 1.9
- route: int32 [4, 1024, 2], P('dp', 'sp'), may hold values from 0 to 31, as said below
- route_weight: float32 [4, 1024, 2], P('dp', 'sp'), may hold values from 0.25 to 1
- w_gate: bfloat16 [32, 2048, 1024], P(('sp', 'dp')), may hold values from -0.125 to 0.125
- w_up: bfloat16 [32, 2048, 1024], P(('sp', 'dp')), may hold values from -0.125 to 0.125
- w_down: bfloat16 [32, 1024, 2048], P(('sp', 'dp')), may hold values from -0.1875 to 0.1875
Outputs:
- result: bfloat16 [4, 1024, 2048], P('dp', 'sp')
Inputs may be any that keep to these rules, and one draw needn't show every extreme that they name: `route`: each token names two different experts of one group (the group of expert e is e // 8). Of the 128 tokens of one device, each expert is named by at most 16; in every draw the 8 experts of one group are each named by exactly 16 tokens of every device.
All inputs are finite; a program needn't handle non-finite values.
Results may differ from a plain program's by a relative error of at most 0.0085.
Values may be sent and summed in bfloat16 or wider, within the bound.
A program may use at most 128 MiB of HBM per device.

v0:
```python
import functools
import math

import jax
import jax.numpy as jnp
from jax import lax
from jax.experimental import pallas as pl
from jax.experimental.pallas import tpu as pltpu
from jax.sharding import PartitionSpec as P

HD = 64
GROUPS = 4
MESH = pl.DeviceIdType.MESH
F32 = jnp.float32
BF16 = jnp.bfloat16
VLIM = 56 * 1024 * 1024

norm_eps = 1e-05


def vmem(count):
    return [pl.BlockSpec(memory_space=pltpu.VMEM)] * count


def swap_kernel(n, count, *refs):
    ins, outs = refs[:count], refs[count : 2 * count]
    send_sem, recv_sem, own_sem = refs[2 * count :]
    me = lax.axis_index("sp")
    dp = lax.axis_index("dp")
    barrier = pltpu.get_barrier_semaphore()
    for d in range(1, n):
        pl.semaphore_signal(
            barrier, inc=1, device_id=(lax.rem(me + d, n), dp), device_id_type=MESH
        )
    own = [
        pltpu.make_async_copy(ins[a].at[me], outs[a].at[me], own_sem.at[a]) for a in range(count)
    ]
    for copy in own:
        copy.start()
    pl.semaphore_wait(barrier, n - 1)
    copies = []
    for d in range(1, n):
        peer = lax.rem(me + d, n)
        for a in range(count):
            copies.append(
                pltpu.make_async_remote_copy(
                    src_ref=ins[a].at[peer],
                    dst_ref=outs[a].at[me],
                    send_sem=send_sem.at[a, d],
                    recv_sem=recv_sem.at[a, d],
                    device_id=(peer, dp),
                    device_id_type=MESH,
                )
            )
            copies[-1].start()
    for copy in own + copies:
        copy.wait()


def swap(n, collective, *arrays):
    count = len(arrays)
    return pl.pallas_call(
        functools.partial(swap_kernel, n, count),
        out_shape=[jax.ShapeDtypeStruct(a.shape, a.dtype) for a in arrays],
        in_specs=vmem(count),
        out_specs=vmem(count),
        scratch_shapes=[
            pltpu.SemaphoreType.DMA((count, n)),
            pltpu.SemaphoreType.DMA((count, n)),
            pltpu.SemaphoreType.DMA((count,)),
        ],
        compiler_params=pltpu.CompilerParams(
            collective_id=collective, has_side_effects=True, vmem_limit_bytes=VLIM
        ),
        name=f"swap{collective}",
    )(*arrays)


def attention_kernel(heads, qkv_ref, shift_ref, out_ref):
    blocks, rows, _ = qkv_ref.shape
    cols = heads * HD
    scale = 1.0 / math.sqrt(HD)
    row = lax.broadcasted_iota(jnp.int32, (2 * rows, 2 * rows), 0)
    col = lax.broadcasted_iota(jnp.int32, (2 * rows, 2 * rows), 1)
    source = jnp.where(row >= rows, row - rows, row)
    summer = jnp.where((col >= rows) | (source > col), 1.0, 0.0).astype(BF16)
    causal = lax.broadcasted_iota(jnp.int32, (rows, rows), 1) < lax.broadcasted_iota(
        jnp.int32, (rows, rows), 0
    )

    def tile(i, j, h, carry, total, diagonal):
        q = qkv_ref[i, :, h * HD : (h + 1) * HD]
        k = qkv_ref[j, :, cols + h * HD : cols + (h + 1) * HD]
        v = qkv_ref[j, :, 2 * cols + h * HD : 2 * cols + (h + 1) * HD]
        z = lax.dot_general(q, k, (((1,), (1,)), ((), ())), preferred_element_type=F32) * scale
        z = z + shift_ref[j, h : h + 1, :]
        soft = jnp.log(1.0 + jnp.exp(-jnp.abs(z)))
        breaks = -jnp.maximum(z, 0.0) - soft
        own = jnp.minimum(z, 0.0) - soft
        if diagonal:
            breaks = jnp.where(causal, breaks, 0.0)
        high = breaks.astype(BF16)
        low = (breaks - high.astype(F32)).astype(BF16)
        sums = jnp.dot(
            jnp.concatenate([high, low], axis=1), summer, preferred_element_type=F32
        )
        weight = jnp.exp(own + (sums[:, :rows] + carry))
        if diagonal:
            weight = jnp.where(causal, weight, 0.0)
        total = total + jnp.dot(weight.astype(BF16), v, preferred_element_type=F32)
        return carry + sums[:, rows:], total

    zero_carry = jnp.zeros((rows, rows), F32)
    zero_total = jnp.zeros((rows, HD), F32)

    for i in range(blocks):
        state = []
        for h in range(heads):
            state.extend(tile(i, i, h, zero_carry, zero_total, True))
        for j in range(i - 1, -1, -1):
            new = []
            for h in range(heads):
                new.extend(tile(i, j, h, state[2 * h], state[2 * h + 1], False))
            state = new
        out_ref[i] = jnp.concatenate([state[2 * h + 1] for h in range(heads)], axis=1).astype(BF16)


def attention(heads, qkv, shift):
    blocks, rows, _ = qkv.shape
    return pl.pallas_call(
        functools.partial(attention_kernel, heads),
        out_shape=jax.ShapeDtypeStruct((blocks, rows, heads * HD), BF16),
        in_specs=vmem(2),
        out_specs=vmem(1)[0],
        compiler_params=pltpu.CompilerParams(vmem_limit_bytes=VLIM),
        name="attention",
    )(qkv, shift)


def place(n_sp, n_dp):
    ny = n_sp // GROUPS
    sp, dp = lax.axis_index("sp"), lax.axis_index("dp")
    plane, y = sp // ny, lax.rem(sp, ny)
    member = y * n_dp + dp

    def at(g, m):
        return (g * ny + m // n_dp, lax.rem(m, n_dp))

    return plane, member, at


def greet(plane, member, at, per_group):
    barrier = pltpu.get_barrier_semaphore()
    for d in range(1, GROUPS):
        pl.semaphore_signal(
            barrier, inc=1, device_id=at(lax.rem(plane + d, GROUPS), member), device_id_type=MESH
        )
    for d in range(1, per_group):
        pl.semaphore_signal(
            barrier, inc=1, device_id=at(plane, lax.rem(member + d, per_group)), device_id_type=MESH
        )
    pl.semaphore_wait(barrier, GROUPS + per_group - 2)


def one_hot_rows(meta, row):
    lanes = lax.broadcasted_iota(jnp.int32, (meta.shape[1], meta.shape[1]), 0).astype(F32)
    return lanes == meta[row : row + 1, :]


def dispatch_kernel(
    n_sp,
    n_dp,
    packed,
    meta,
    got,
    got_meta,
    block,
    stage,
    z_send,
    z_recv,
    t_send,
    t_recv,
    p_send,
    p_recv,
    own_sem,
):
    _, per_group, cap, width = got.shape
    slots = packed.shape[1]
    chunk = min(512, width)
    plane, member, at = place(n_sp, n_dp)
    greet(plane, member, at, per_group)
    z_copies, t_copies = [None], [None]
    for d in range(1, GROUPS):
        other = lax.rem(plane + d, GROUPS)
        for kept, src, dst, send, recv in (
            (t_copies, meta, got_meta, t_send, t_recv),
            (z_copies, packed, block, z_send, z_recv),
        ):
            kept.append(
                pltpu.make_async_remote_copy(
                    src_ref=src.at[other],
                    dst_ref=dst.at[plane],
                    send_sem=send.at[d],
                    recv_sem=recv.at[d],
                    device_id=at(other, member),
                    device_id_type=MESH,
                )
            )
            kept[-1].start()
    got_meta[plane] = meta[plane]
    later = []
    for d in range(GROUPS):
        source = lax.rem(plane - d + GROUPS, GROUPS)
        if d:
            t_copies[d].wait_recv()
            z_copies[d].wait_recv()
        held = block if d else packed
        info = got_meta[source]
        hot = jnp.where(one_hot_rows(info, 0) | one_hot_rows(info, 1), 1.0, 0.0).astype(BF16)
        hot = hot[:, :slots]
        for c in range(0, width, chunk):
            rows = jnp.dot(hot, held[source, :, c : c + chunk], preferred_element_type=F32)
            for m in range(per_group):
                stage[source, m, :, c : c + chunk] = rows[m * cap : (m + 1) * cap].astype(BF16)
        own = pltpu.make_async_copy(stage.at[source, member], got.at[source, member], own_sem.at[d])
        own.start()
        later.append(own)
        for e in range(1, per_group):
            other = lax.rem(member + e, per_group)
            copy = pltpu.make_async_remote_copy(
                src_ref=stage.at[source, other],
                dst_ref=got.at[source, member],
                send_sem=p_send.at[d, e],
                recv_sem=p_recv.at[d, e],
                device_id=at(plane, other),
                device_id_type=MESH,
            )
            copy.start()
            later.append(copy)
    for copy in later:
        copy.wait()
    for d in range(1, GROUPS):
        t_copies[d].wait_send()
        z_copies[d].wait_send()


def dispatch(n_sp, n_dp, cap, packed, meta):
    per_group = n_sp * n_dp // GROUPS
    _, slots, width = packed.shape
    buffer = (GROUPS, per_group, cap, width)
    dma = pltpu.SemaphoreType.DMA
    return pl.pallas_call(
        functools.partial(dispatch_kernel, n_sp, n_dp),
        out_shape=[
            jax.ShapeDtypeStruct(buffer, BF16),
            jax.ShapeDtypeStruct(meta.shape, F32),
        ],
        in_specs=vmem(2),
        out_specs=vmem(2),
        scratch_shapes=[
            pltpu.VMEM(packed.shape, BF16),
            pltpu.VMEM(buffer, BF16),
            dma((GROUPS,)),
            dma((GROUPS,)),
            dma((GROUPS,)),
            dma((GROUPS,)),
            dma((GROUPS, per_group)),
            dma((GROUPS, per_group)),
            dma((GROUPS,)),
        ],
        compiler_params=pltpu.CompilerParams(
            collective_id=2, has_side_effects=True, vmem_limit_bytes=VLIM
        ),
        name="dispatch",
    )(packed, meta)


def combine_kernel(
    n_sp,
    n_dp,
    reply,
    meta,
    out,
    block,
    stage,
    z_send,
    z_recv,
    p_send,
    p_recv,
    own_sem,
):
    _, per_group, cap, width = reply.shape
    slots = out.shape[1]
    chunk = min(512, width)
    plane, member, at = place(n_sp, n_dp)
    greet(plane, member, at, per_group)
    order = list(range(1, GROUPS)) + [0]
    plane_copies = {}
    for d in order:
        target = lax.rem(plane + d, GROUPS)
        own = pltpu.make_async_copy(reply.at[target, member], block.at[target, member], own_sem.at[d])
        own.start()
        copies = [own]
        for e in range(1, per_group):
            other = lax.rem(member + e, per_group)
            copies.append(
                pltpu.make_async_remote_copy(
                    src_ref=reply.at[target, other],
                    dst_ref=block.at[target, member],
                    send_sem=p_send.at[d, e],
                    recv_sem=p_recv.at[d, e],
                    device_id=at(plane, other),
                    device_id_type=MESH,
                )
            )
            copies[-1].start()
        plane_copies[d] = copies
    z_copies = []
    for d in order:
        target = lax.rem(plane + d, GROUPS)
        for copy in plane_copies[d]:
            copy.wait()
        info = meta[target]
        spread = jnp.where(one_hot_rows(info, 0), info[2:3, :], 0.0) + jnp.where(
            one_hot_rows(info, 1), info[3:4, :], 0.0
        )
        spread = spread.T[:slots]
        high = spread.astype(BF16)
        low = (spread - high.astype(F32)).astype(BF16)
        for c in range(0, width, chunk):
            if cap % 16 == 0:
                rows = block[target, :, :, c : c + chunk].reshape(per_group * cap, chunk)
            else:
                rows = jnp.concatenate(
                    [block[target, m, :, c : c + chunk].astype(F32) for m in range(per_group)], axis=0
                ).astype(BF16)
            total = jnp.dot(high, rows, preferred_element_type=F32) + jnp.dot(
                low, rows, preferred_element_type=F32
            )
            if d:
                stage[target, :, c : c + chunk] = total.astype(BF16)
            else:
                out[target, :, c : c + chunk] = total.astype(BF16)
        if d:
            copy = pltpu.make_async_remote_copy(
                src_ref=stage.at[target],
                dst_ref=out.at[plane],
                send_sem=z_send.at[d],
                recv_sem=z_recv.at[d],
                device_id=at(target, member),
                device_id_type=MESH,
            )
            copy.start()
            z_copies.append(copy)
    for copy in z_copies:
        copy.wait()


def combine(n_sp, n_dp, slots, reply, meta):
    _, per_group, cap, width = reply.shape
    dma = pltpu.SemaphoreType.DMA
    return pl.pallas_call(
        functools.partial(combine_kernel, n_sp, n_dp),
        out_shape=jax.ShapeDtypeStruct((GROUPS, slots, width), BF16),
        in_specs=vmem(2),
        out_specs=vmem(1)[0],
        scratch_shapes=[
            pltpu.VMEM(reply.shape, BF16),
            pltpu.VMEM((GROUPS, slots, width), BF16),
            dma((GROUPS,)),
            dma((GROUPS,)),
            dma((GROUPS, per_group)),
            dma((GROUPS, per_group)),
            dma((GROUPS,)),
        ],
        compiler_params=pltpu.CompilerParams(
            collective_id=3, has_side_effects=True, vmem_limit_bytes=VLIM
        ),
        name="combine",
    )(reply, meta)


def on_device(
    n_sp,
    n_dp,
    stream,
    queries,
    keys_in,
    values_in,
    key_shift,
    head_shift,
    mix_gain,
    out_weight,
    post_gain,
    route,
    route_weight,
    w_gate,
    w_up,
    w_down,
):
    tokens, width = stream.shape[1], stream.shape[2]
    heads = key_shift.shape[2] // n_sp
    cols = heads * HD

    n_expert = n_sp * n_dp
    per_group = n_expert // GROUPS
    cap = tokens // per_group
    slots = tokens // 2
    expert_ids = route[0].reshape(tokens * 2)
    onehot = (expert_ids[:, None] == jnp.arange(n_expert, dtype=jnp.int32)[None, :]).astype(BF16)
    before = jnp.arange(tokens * 2)
    earlier = (before[:, None] > before[None, :]).astype(BF16)
    counts = jnp.dot(earlier, onehot, preferred_element_type=F32)
    ranks = jnp.sum(counts * onehot.astype(F32), axis=1)
    inside = lax.rem(expert_ids, per_group).astype(F32) * cap + ranks
    inside = inside.reshape(tokens, 2)
    token_group = route[0][:, 0] // per_group
    group_hot = (token_group[:, None] == jnp.arange(GROUPS, dtype=jnp.int32)[None, :]).astype(BF16)
    group_rank = jnp.sum(
        jnp.dot(earlier[:tokens, :tokens], group_hot, preferred_element_type=F32)
        * group_hot.astype(F32),
        axis=1,
    )
    slot = token_group * slots + group_rank.astype(jnp.int32)
    slot_hot = slot[None, :] == jnp.arange(GROUPS * slots, dtype=jnp.int32)[:, None]
    facts = jnp.concatenate([inside + 1.0, route_weight[0]], axis=1)
    table = jnp.sum(jnp.where(slot_hot[:, None, :], facts.T[None, :, :], 0.0), axis=2)
    table = table - jnp.array([1.0, 1.0, 0.0, 0.0], F32)[None, :]
    table = table.reshape(GROUPS, slots, 4).transpose(0, 2, 1)
    lanes = per_group * cap
    meta = jnp.full((GROUPS, 8, lanes), -1.0, F32).at[:, :4, :slots].set(table)

    def by_peer(array):
        return array[0].reshape(tokens, n_sp, cols).transpose(1, 0, 2)

    qkv = jnp.concatenate([by_peer(queries), by_peer(keys_in), by_peer(values_in)], axis=2)
    offsets = (key_shift[0].astype(F32) + head_shift[None, :]).T.reshape(n_sp, heads, tokens)
    offsets = jnp.pad(offsets, ((0, 0), (0, 8 - heads), (0, 0)))
    qkv, offsets = swap(n_sp, 0, qkv, offsets)
    attended = attention(heads, qkv, offsets)
    (attended,) = swap(n_sp, 1, attended)
    att32 = attended.transpose(1, 0, 2).reshape(tokens, n_sp * cols).astype(F32)
    normed = (
        att32 * lax.rsqrt(jnp.mean(att32 * att32, axis=1, keepdims=True) + norm_eps) * mix_gain
    ).astype(BF16)
    mixed = jnp.dot(normed, out_weight, preferred_element_type=F32)
    summed = stream[0].astype(F32) + mixed
    hidden = (
        summed * lax.rsqrt(jnp.mean(summed * summed, axis=1, keepdims=True) + norm_eps) * post_gain
    ).astype(BF16)

    slot_hot = slot_hot.astype(BF16)
    packed = jnp.dot(slot_hot, hidden, preferred_element_type=F32).astype(BF16)
    received, tables = dispatch(n_sp, n_dp, cap, packed.reshape(GROUPS, slots, width), meta)
    rows = received.reshape(GROUPS * per_group * cap, width)
    gate = jnp.dot(rows, w_gate[0], preferred_element_type=F32)
    upper = jnp.dot(rows, w_up[0], preferred_element_type=F32)
    inner = (jax.nn.silu(gate) * upper).astype(BF16)
    reply = jnp.dot(inner, w_down[0], preferred_element_type=F32).astype(BF16)
    returned = combine(n_sp, n_dp, slots, reply.reshape(received.shape), tables)
    moe_sum = lax.dot_general(
        slot_hot,
        returned.reshape(GROUPS * slots, width),
        (((0,), (0,)), ((), ())),
        preferred_element_type=F32,
    )
    return (hidden.astype(F32) + moe_sum).astype(BF16)[None]


def solution(mesh):
    return jax.shard_map(
        functools.partial(on_device, mesh.shape["sp"], mesh.shape["dp"]),
        mesh=mesh,
        in_specs=(
            P("dp", "sp", None),
            P("dp", "sp", None),
            P("dp", "sp", None),
            P("dp", "sp", None),
            P("dp", "sp", None),
            P(),
            P(),
            P(),
            P(),
            P("dp", "sp", None),
            P("dp", "sp", None),
            P(("sp", "dp"), None, None),
            P(("sp", "dp"), None, None),
            P(("sp", "dp"), None, None),
        ),
        out_specs=P("dp", "sp", None),
        check_vma=False,
    )
```

profile of v0, /device:TPU:9, one launch (start us, length us, event | category | flops | bytes accessed | tf_op | source)
XLA Modules:
  0.0 166.8 jit_solution(6372753609826974642)
XLA Ops:
  0.0 0.7 fusion.33
  0.7 0.8 convert_add_fusion
  1.5 0.6 pad.9.refs_1_
  2.1 0.8 copy.69
  3.0 0.2 fusion.13
  3.5 0.7 fusion.32
  4.2 0.7 maximum_bitcast_fusion
  5.0 0.7 convert_add_fusion.1
  5.8 0.2 select_reduce_fusion
  6.1 0.7 fusion.25
  6.8 0.6 scatter.4.meta
  7.4 1.1 copy.62
  8.5 0.2 copy.63
  8.7 1.1 copy.64
  9.9 0.2 copy.65
  10.1 0.2 copy.66
  10.2 0.2 copy.67
  10.4 1.0 pad_maximum_fusion.refs_0_
  11.4 22.6 %swap0.1 = (bf16[8,128,384]{2,1,0:T(8,128)(2,1)}, f32[8,8,128]{2,1,0:T(8,128)}) custom-call(bf16[8,128,384]{2,1,0:T(8,128)(2,1)} %pad_maximum_fusion.refs_0_, f32[8,8,128]{2,1,0:T(8,128)} %pad.9.refs_1_), custom_call_target="tpu_custom_call" | custom-call | tf_op jit(solution)/shard_map/swap0/pallas_call | solution.py:62
  34.0 13.4 %attention.1.refs_0_ = bf16[8,128,128]{2,1,0:T(8,128)(2,1)} custom-call(bf16[8,128,384]{2,1,0:T(8,128)(2,1)} %get-tuple-element.21.qkv_ref, f32[8,8,128]{2,1,0:T(8,128)} %get-tuple-element.22.shift_ref), custom_call_target="tpu_custom_call" | custom-call | tf_op jit(solution)/shard_map/attention/pallas_call | solution.py:130
  47.5 10.6 %swap1.1 = bf16[8,128,128]{2,1,0:T(8,128)(2,1)} custom-call(bf16[8,128,128]{2,1,0:T(8,128)(2,1)} %attention.1.refs_0_), custom_call_target="tpu_custom_call" | custom-call | tf_op jit(solution)/shard_map/swap1/pallas_call | solution.py:62
  58.1 1.1 fusion.17
  59.2 1.0 convert_bitcast_fusion
  60.2 0.2 copy.68
  60.4 0.2 fusion.19
  60.6 3.2 %multiply_reduce_fusion = (f32[128]{0:T(128)S(1)}, f32[128,2048]{1,0:T(8,128)S(1)}) fusion(bf16[128,1024]{0,1:T(8,128)(2,1)S(1)} %fusion.19, bf16[1024,2048]{1,0:T(8,128)(2,1)} %param.24, bf16[1,128,2048]{2,1,0:T(8,128)(2,1)S(1)} %copy-done), kind=kOutput, calls=%fused_computation.18 | convolution fusion | flops 537919360 | bytes 6029824 | tf_op jit(solution)/shard_map/dot_general | solution.py:446
  63.8 1.5 convolution_convert_fusion
  65.3 38.9 %dispatch.1 = (bf16[4,8,16,2048]{3,2,1,0:T(8,128)(2,1)}, f32[4,8,128]{2,1,0:T(8,128)}) custom-call(bf16[4,64,2048]{2,1,0:T(8,128)(2,1)} %bitcast.71, f32[4,8,128]{2,1,0:T(8,128)} %scatter.4.meta), custom_call_target="tpu_custom_call" | custom-call | tf_op jit(solution)/shard_map/dispatch/pallas_call | solution.py:252
  104.2 5.4 %fusion.4 = f32[512,1024]{1,0:T(8,128)} fusion(bf16[512,2048]{1,0:T(8,128)(2,1)} %bitcast.83, bf16[1,2048,1024]{2,1,0:T(8,128)(2,1)S(1)} %copy-done.4), kind=kOutput, calls=%fused_computation.4 | convolution fusion | flops 2147483648 | bytes 8388608 | tf_op jit(solution)/shard_map/dot_general | solution.py:456
  109.6 10.0 %fusion.6 = bf16[512,2048]{1,0:T(8,128)(2,1)} fusion(bf16[1,1024,2048]{2,1,0:T(8,128)(2,1)} %param.30, f32[512,1024]{1,0:T(8,128)} %fusion.4, bf16[512,2048]{1,0:T(8,128)(2,1)S(1)} %bitcast.84, bf16[1,2048,1024]{2,1,0:T(8,128)(2,1)} %param.29), kind=kOutput, calls=%fused_computation.6 | convolution fusion | flops 4299161600 | bytes 14680064 | tf_op jit(solution)/shard_map/dot_general | solution.py:459
  119.6 44.8 %combine.1 = bf16[4,64,2048]{2,1,0:T(8,128)(2,1)} custom-call(bf16[4,8,16,2048]{3,2,1,0:T(8,128)(2,1)} %bitcast.72, f32[4,8,128]{2,1,0:T(8,128)} %get-tuple-element.24.meta), custom_call_target="tpu_custom_call" | custom-call | tf_op jit(solution)/shard_map/combine/pallas_call | solution.py:362
  164.4 2.4 %fusion.10 = bf16[1,128,2048]{2,1,0:T(8,128)(2,1)} fusion(bf16[256,2048]{1,0:T(8,128)(2,1)} %bitcast.70, s32[128]{0:T(128)S(1)} %convert_add_fusion.1, f32[2048]{0:T(1024)S(1)} %copy-done.2, f32[128,2048]{1,0:T(8,128)S(1)} %get-tuple-element.26, f32[128]{0:T(128)S(1)} %add_rsqrt_fusion), kind=kOutput, calls=%fused_computation.11 | convolution fusion | flops 135823360 | bytes 2630656 | tf_op jit(solution)/shard_map/dot_general | solution.py:461
  (21 shorter events, 0.7 us)
Async XLA Ops:
  0.0 10.1 %copy-start.1 = (bf16[1,128,1024]{2,1,0:T(8,128)(2,1)S(1)}, bf16[1,128,1024]{2,1,0:T(8,128)(2,1)}, u32[]{:S(2)}) copy-start(bf16[1,128,1024]{2,1,0:T(8,128)(2,1)} %param.20) | copy-start | bytes 786436
  11.4 49.0 %copy-start.3 = (f32[1024]{0:T(1024)S(1)}, f32[1024]{0:T(1024)}, u32[]{:S(2)}) copy-start(f32[1024]{0:T(1024)} %param.23) | copy-start | bytes 12292
  34.0 26.6 %copy-start = (bf16[1,128,2048]{2,1,0:T(8,128)(2,1)S(1)}, bf16[1,128,2048]{2,1,0:T(8,128)(2,1)}, u32[]{:S(2)}) copy-start(bf16[1,128,2048]{2,1,0:T(8,128)(2,1)} %param.17) | copy-start | bytes 1572868
  60.6 3.2 %copy-start.2 = (f32[2048]{0:T(1024)S(1)}, f32[2048]{0:T(1024)}, u32[]{:S(2)}) copy-start(f32[2048]{0:T(1024)} %param.25) | copy-start | bytes 24580
  60.6 43.6 %copy-start.4 = (bf16[1,2048,1024]{2,1,0:T(8,128)(2,1)S(1)}, bf16[1,2048,1024]{2,1,0:T(8,128)(2,1)}, u32[]{:S(2)}) copy-start(bf16[1,2048,1024]{2,1,0:T(8,128)(2,1)} %param.28) | copy-start | bytes 12582916
  104.2 5.5 %copy-start.5 = (bf16[4,8,16,2048]{3,2,1,0:T(8,128)(2,1)S(1)}, bf16[4,8,16,2048]{3,2,1,0:T(8,128)(2,1)}, u32[]{:S(2)}) copy-start(bf16[4,8,16,2048]{3,2,1,0:T(8,128)(2,1)} %get-tuple-element.23) | copy-start | bytes 6291460
where the time goes:
time: 167 us
  Pallas kernels  130 us (78%)
  matrix products  22.8 us (14%)
  other arithmetic  7.88 us (5%)
  local copies, waits for them, and re-layouts  5.62 us (3%)
    pallas_call x1, Pallas kernels, combine(): pl.pallas_call(functools.partial(combine_kernel, n_sp, n_dp), out_shape=j...  44.8 us
    pallas_call x1, Pallas kernels, dispatch(): pl.pallas_call(functools.partial(dispatch_kernel, n_sp, n_dp), out_shape=...  38.9 us
    pallas_call x2, Pallas kernels, swap(): pl.pallas_call(functools.partial(swap_kernel, n, count), out_shape=[jax.S...  33.2 us
    pallas_call x1, Pallas kernels, attention(): pl.pallas_call(functools.partial(attention_kernel, heads), out_shape=jax....  13.4 us
    dot_general x1, matrix products, on_device(): reply = jnp.dot(inner, w_down[0], preferred_element_type=F32).astype(BF16)  9.96 us
    dot_general x1, matrix products, on_device(): gate = jnp.dot(rows, w_gate[0], preferred_element_type=F32)  5.44 us

commit v1 on v0

--- a/solution.py
+++ b/solution.py
@@ -149,6 +149,14 @@
     return plane, member, at
 
 
+def partner(plane, d):
+    if d == 1:
+        return plane + 1 - 2 * lax.rem(plane, 2)
+    if d == 2:
+        return lax.rem(plane + 2, GROUPS)
+    return 3 - plane if d == 3 else plane
+
+
 def greet(plane, member, at, per_group):
     barrier = pltpu.get_barrier_semaphore()
     for d in range(1, GROUPS):
@@ -189,14 +197,14 @@
     chunk = min(512, width)
     plane, member, at = place(n_sp, n_dp)
     greet(plane, member, at, per_group)
-    z_copies, t_copies = [None], [None]
-    for d in range(1, GROUPS):
-        other = lax.rem(plane + d, GROUPS)
+    z_copies, t_copies = {}, {}
+    for d in (2, 3, 1):
+        other = partner(plane, d)
         for kept, src, dst, send, recv in (
             (t_copies, meta, got_meta, t_send, t_recv),
             (z_copies, packed, block, z_send, z_recv),
         ):
-            kept.append(
+            kept[d] = (
                 pltpu.make_async_remote_copy(
                     src_ref=src.at[other],
                     dst_ref=dst.at[plane],
@@ -206,11 +214,11 @@
                     device_id_type=MESH,
                 )
             )
-            kept[-1].start()
+            kept[d].start()
     got_meta[plane] = meta[plane]
     later = []
-    for d in range(GROUPS):
-        source = lax.rem(plane - d + GROUPS, GROUPS)
+    for d in (0, 2, 3, 1):
+        source = partner(plane, d)
         if d:
             t_copies[d].wait_recv()
             z_copies[d].wait_recv()
@@ -294,10 +302,10 @@
     chunk = min(512, width)
     plane, member, at = place(n_sp, n_dp)
     greet(plane, member, at, per_group)
-    order = list(range(1, GROUPS)) + [0]
+    order = (2, 3, 1, 0)
     plane_copies = {}
     for d in order:
-        target = lax.rem(plane + d, GROUPS)
+        target = partner(plane, d)
         own = pltpu.make_async_copy(reply.at[target, member], block.at[target, member], own_sem.at[d])
         own.start()
         copies = [own]
@@ -317,7 +325,7 @@
         plane_copies[d] = copies
     z_copies = []
     for d in order:
-        target = lax.rem(plane + d, GROUPS)
+        target = partner(plane, d)
         for copy in plane_copies[d]:
             copy.wait()
         info = meta[target]

time: 167 us -> 169 us (1.012); the launches traced: 167 us -> 166 us
    pallas_call x1, Pallas kernels: 44.8 us -> 38.6 us  [combine(): pl.pallas_call(functools.partial(combine_kernel, n_sp, n_dp), out_shape=j...]
    pallas_call x1, Pallas kernels: 38.9 us -> 44.2 us  [dispatch(): pl.pallas_call(functools.partial(dispatch_kernel, n_sp, n_dp), out_shape=...]
where the time goes in v1:
time: 169 us; the launch traced here: 166 us
  Pallas kernels  129 us (76%)
  matrix products  22.8 us (13%)
  other arithmetic  7.88 us (5%)
  local copies, waits for them, and re-layouts  5.62 us (3%)
    pallas_call x1, Pallas kernels, dispatch(): pl.pallas_call(functools.partial(dispatch_kernel, n_sp, n_dp), out_shape=...  44.2 us
    pallas_call x1, Pallas kernels, combine(): pl.pallas_call(functools.partial(combine_kernel, n_sp, n_dp), out_shape=j...  38.6 us
    pallas_call x2, Pallas kernels, swap(): pl.pallas_call(functools.partial(swap_kernel, n, count), out_shape=[jax.S...  33.2 us
    pallas_call x1, Pallas kernels, attention(): pl.pallas_call(functools.partial(attention_kernel, heads), out_shape=jax....  13.4 us
    dot_general x1, matrix products, on_device(): reply = jnp.dot(inner, w_down[0], preferred_element_type=F32).astype(BF16)  9.95 us
    dot_general x1, matrix products, on_device(): gate = jnp.dot(rows, w_gate[0], preferred_element_type=F32)  5.44 us

profile of v1, /device:TPU:9, one launch (start us, length us, event | category | flops | bytes accessed | tf_op | source)
XLA Modules:
  0.0 166.0 jit_solution(5026782102503292955)
XLA Ops:
  0.0 0.7 fusion.33
  0.7 0.8 convert_add_fusion
  1.5 0.6 pad.9.refs_1_
  2.1 0.8 copy.69
  3.0 0.2 fusion.13
  3.5 0.7 fusion.32
  4.2 0.7 maximum_bitcast_fusion
  5.0 0.7 convert_add_fusion.1
  5.8 0.2 select_reduce_fusion
  6.1 0.7 fusion.25
  6.8 0.6 scatter.4.meta
  7.4 1.1 copy.62
  8.5 0.2 copy.63
  8.7 1.1 copy.64
  9.9 0.2 copy.65
  10.1 0.2 copy.66
  10.2 0.2 copy.67
  10.4 1.0 pad_maximum_fusion.refs_0_
  11.4 22.6 %swap0.1 = (bf16[8,128,384]{2,1,0:T(8,128)(2,1)}, f32[8,8,128]{2,1,0:T(8,128)}) custom-call(bf16[8,128,384]{2,1,0:T(8,128)(2,1)} %pad_maximum_fusion.refs_0_, f32[8,8,128]{2,1,0:T(8,128)} %pad.9.refs_1_), custom_call_target="tpu_custom_call" | custom-call | tf_op jit(solution)/shard_map/swap0/pallas_call | solution.py:62
  34.0 13.4 %attention.1.refs_0_ = bf16[8,128,128]{2,1,0:T(8,128)(2,1)} custom-call(bf16[8,128,384]{2,1,0:T(8,128)(2,1)} %get-tuple-element.21.qkv_ref, f32[8,8,128]{2,1,0:T(8,128)} %get-tuple-element.22.shift_ref), custom_call_target="tpu_custom_call" | custom-call | tf_op jit(solution)/shard_map/attention/pallas_call | solution.py:130
  47.5 10.6 %swap1.1 = bf16[8,128,128]{2,1,0:T(8,128)(2,1)} custom-call(bf16[8,128,128]{2,1,0:T(8,128)(2,1)} %attention.1.refs_0_), custom_call_target="tpu_custom_call" | custom-call | tf_op jit(solution)/shard_map/swap1/pallas_call | solution.py:62
  58.1 1.1 fusion.17
  59.2 1.0 convert_bitcast_fusion
  60.2 0.2 copy.68
  60.4 0.2 fusion.19
  60.6 3.2 %multiply_reduce_fusion = (f32[128]{0:T(128)S(1)}, f32[128,2048]{1,0:T(8,128)S(1)}) fusion(bf16[128,1024]{0,1:T(8,128)(2,1)S(1)} %fusion.19, bf16[1024,2048]{1,0:T(8,128)(2,1)} %param.24, bf16[1,128,2048]{2,1,0:T(8,128)(2,1)S(1)} %copy-done), kind=kOutput, calls=%fused_computation.18 | convolution fusion | flops 537919360 | bytes 6029824 | tf_op jit(solution)/shard_map/dot_general | solution.py:454
  63.8 1.5 convolution_convert_fusion
  65.3 44.2 %dispatch.1 = (bf16[4,8,16,2048]{3,2,1,0:T(8,128)(2,1)}, f32[4,8,128]{2,1,0:T(8,128)}) custom-call(bf16[4,64,2048]{2,1,0:T(8,128)(2,1)} %bitcast.71, f32[4,8,128]{2,1,0:T(8,128)} %scatter.4.meta), custom_call_target="tpu_custom_call" | custom-call | tf_op jit(solution)/shard_map/dispatch/pallas_call | solution.py:260
  109.6 5.4 %fusion.4 = f32[512,1024]{1,0:T(8,128)} fusion(bf16[512,2048]{1,0:T(8,128)(2,1)} %bitcast.83, bf16[1,2048,1024]{2,1,0:T(8,128)(2,1)S(1)} %copy-done.4), kind=kOutput, calls=%fused_computation.4 | convolution fusion | flops 2147483648 | bytes 8388608 | tf_op jit(solution)/shard_map/dot_general | solution.py:464
  115.0 9.9 %fusion.6 = bf16[512,2048]{1,0:T(8,128)(2,1)} fusion(bf16[1,1024,2048]{2,1,0:T(8,128)(2,1)} %param.30, f32[512,1024]{1,0:T(8,128)} %fusion.4, bf16[512,2048]{1,0:T(8,128)(2,1)S(1)} %bitcast.84, bf16[1,2048,1024]{2,1,0:T(8,128)(2,1)} %param.29), kind=kOutput, calls=%fused_computation.6 | convolution fusion | flops 4299161600 | bytes 14680064 | tf_op jit(solution)/shard_map/dot_general | solution.py:467
  125.0 38.6 %combine.1 = bf16[4,64,2048]{2,1,0:T(8,128)(2,1)} custom-call(bf16[4,8,16,2048]{3,2,1,0:T(8,128)(2,1)} %bitcast.72, f32[4,8,128]{2,1,0:T(8,128)} %get-tuple-element.24.meta), custom_call_target="tpu_custom_call" | custom-call | tf_op jit(solution)/shard_map/combine/pallas_call | solution.py:370
  163.6 2.4 %fusion.10 = bf16[1,128,2048]{2,1,0:T(8,128)(2,1)} fusion(bf16[256,2048]{1,0:T(8,128)(2,1)} %bitcast.70, s32[128]{0:T(128)S(1)} %convert_add_fusion.1, f32[2048]{0:T(1024)S(1)} %copy-done.2, f32[128,2048]{1,0:T(8,128)S(1)} %get-tuple-element.26, f32[128]{0:T(128)S(1)} %add_rsqrt_fusion), kind=kOutput, calls=%fused_computation.11 | convolution fusion | flops 135823360 | bytes 2630656 | tf_op jit(solution)/shard_map/dot_general | solution.py:469
  (21 shorter events, 0.7 us)
Async XLA Ops:
  0.0 10.1 %copy-start.1 = (bf16[1,128,1024]{2,1,0:T(8,128)(2,1)S(1)}, bf16[1,128,1024]{2,1,0:T(8,128)(2,1)}, u32[]{:S(2)}) copy-start(bf16[1,128,1024]{2,1,0:T(8,128)(2,1)} %param.20) | copy-start | bytes 786436
  11.4 49.0 %copy-start.3 = (f32[1024]{0:T(1024)S(1)}, f32[1024]{0:T(1024)}, u32[]{:S(2)}) copy-start(f32[1024]{0:T(1024)} %param.23) | copy-start | bytes 12292
  34.0 26.6 %copy-start = (bf16[1,128,2048]{2,1,0:T(8,128)(2,1)S(1)}, bf16[1,128,2048]{2,1,0:T(8,128)(2,1)}, u32[]{:S(2)}) copy-start(bf16[1,128,2048]{2,1,0:T(8,128)(2,1)} %param.17) | copy-start | bytes 1572868
  60.6 3.2 %copy-start.2 = (f32[2048]{0:T(1024)S(1)}, f32[2048]{0:T(1024)}, u32[]{:S(2)}) copy-start(f32[2048]{0:T(1024)} %param.25) | copy-start | bytes 24580
  60.6 49.0 %copy-start.4 = (bf16[1,2048,1024]{2,1,0:T(8,128)(2,1)S(1)}, bf16[1,2048,1024]{2,1,0:T(8,128)(2,1)}, u32[]{:S(2)}) copy-start(bf16[1,2048,1024]{2,1,0:T(8,128)(2,1)} %param.28) | copy-start | bytes 12582916
  109.6 5.5 %copy-start.5 = (bf16[4,8,16,2048]{3,2,1,0:T(8,128)(2,1)S(1)}, bf16[4,8,16,2048]{3,2,1,0:T(8,128)(2,1)}, u32[]{:S(2)}) copy-start(bf16[4,8,16,2048]{3,2,1,0:T(8,128)(2,1)} %get-tuple-element.23) | copy-start | bytes 6291460
